TPU v7x, 32 devices: a whole 2x2x4 slice. The times are simulated.
32 devices in a mesh: sp: 8 (over z, x), tp: 4 (over y, core).
Axes of the slice: x: 2, y: 2, z: 4, core: 2. Of those that a mesh axis runs over, the one named last changes fastest.
Arguments:
- stream_in: bfloat16 [1024, 2048], P('sp'), may hold values from -8 to 8
- out_cot: bfloat16 [1024, 2048], P('sp'), may hold values from -6 to 6
- route_experts: int32 [1024, 2], P('sp'), may hold values from 0 to 7, all different within a row; in each aligned block of 128 rows (0 to 127, 128 to 255, ...) at most 64 rows name the same one
- route_weights: float32 [1024, 2], P('sp'), may hold values from 0.1 to 1
- w_gate: bfloat16 [8, 2048, 2048], P('sp', None, 'tp'), may hold values from -0.125 to 0.125
- w_up: bfloat16 [8, 2048, 2048], P('sp', None, 'tp'), may hold values from -0.125 to 0.125
- w_down: bfloat16 [8, 2048, 2048], P('sp', 'tp'), may hold values from -0.125 to 0.125
- w_proj: bfloat16 [2048, 1024], P(None, 'tp'), may hold values from -0.1875 to 0.1875
- conv_value: bfloat16 [1024, 1024], P('tp', 'sp'), may hold values from -6 to 6
- conv_gate: bfloat16 [1024, 1024], P('tp', 'sp'), may hold values from -8 to 8
- conv_taps: float32 [31, 1024], P(None, 'tp'), may hold values from -1 to 1
- conv_result: bfloat16 [1024, 1024], P('tp', 'sp'), may hold values from -100 to 100
- channel_norm_gain: float32 [1024], P('tp'), may hold values from 0.1 to 1.9
Outputs:
- grad_gate: bfloat16 [8, 2048, 2048], P('sp', None, 'tp')
- grad_up: bfloat16 [8, 2048, 2048], P('sp', None, 'tp')
- grad_down: bfloat16 [8, 2048, 2048], P('sp', 'tp')
- grad_stream: bfloat16 [1024, 2048], P('sp')
- grad_proj: float32 [2048, 1024], P('sp', 'tp')
- grad_value: bfloat16 [1024, 1024], P('tp', 'sp')
- grad_gate_in: bfloat16 [1024, 1024], P('tp', 'sp')
Inputs may be any that keep to these rules, and one draw needn't show every extreme that they name: `route_experts`: each row names 2 different experts; within each aligned block of 128 rows no expert is named by more than 64 rows, and at least one block reaches that bound for some expert.
All inputs are finite; a program needn't handle non-finite values.
Results may differ from a plain program's by a relative error of at most 0.025.
Values may be sent and summed in bfloat16 or wider, within the bound.
A program may use at most 64 MiB of HBM per device.

v0:
```python
import jax
import jax.numpy as jnp
from jax import lax
from jax.sharding import PartitionSpec as P

norm_eps = 1e-05
clamp_limit = 7.0
alpha_gate = 1.702


def from_behind(value, axis, steps):
    count = lax.axis_size(axis)
    leading, last = (max(0, -steps), min(count, count - steps))
    return lax.ppermute(value, axis, [(source, source + steps) for source in range(leading, last)])


def slot_tables(block_routes, experts_all, capacity):
    flat_routes = block_routes.reshape(-1)
    assigns = flat_routes.shape[0]
    onehot = (flat_routes[:, None] == jnp.arange(experts_all, dtype=jnp.int32)[None, :]).astype(
        jnp.int32
    )
    before = jnp.cumsum(onehot, axis=0) - onehot
    rank_in = jnp.sum(before * onehot, axis=1)
    slot_of = flat_routes * capacity + rank_in
    source_of = (
        jnp.full((experts_all * capacity,), -1, jnp.int32)
        .at[slot_of]
        .set(jnp.arange(assigns, dtype=jnp.int32))
    )
    return (slot_of, source_of)


def combine_routes(returned, slot_of, cot_cols, token_rows, top_count):
    feature_count = returned.shape[-1]
    flat_back = returned.reshape(-1, feature_count)
    per_route = flat_back[slot_of].astype(jnp.float32).reshape(token_rows, top_count, feature_count)
    return (cot_cols.astype(jnp.float32) + jnp.sum(per_route, axis=1)).astype(jnp.bfloat16)


def expert_terms(rows_in, cot_in, w_gate, w_up, w_down):
    pre_gate = jnp.einsum("secd,edf->secf", rows_in, w_gate, preferred_element_type=jnp.float32)
    pre_up = jnp.einsum("secd,edf->secf", rows_in, w_up, preferred_element_type=jnp.float32)
    glu_part = jnp.minimum(pre_gate, clamp_limit)
    lin_part = jnp.clip(pre_up, -clamp_limit, clamp_limit)
    sig_glu = jax.nn.sigmoid(alpha_gate * glu_part)
    activated = (glu_part * sig_glu * (lin_part + 1.0)).astype(jnp.bfloat16)
    grad_act = jnp.einsum("secd,efd->secf", cot_in, w_down, preferred_element_type=jnp.float32)
    slope = sig_glu + alpha_gate * glu_part * sig_glu * (1.0 - sig_glu)
    grad_pre_gate = jnp.where(
        pre_gate < clamp_limit, grad_act * (lin_part + 1.0) * slope, 0.0
    ).astype(jnp.bfloat16)
    grad_pre_up = jnp.where(
        jnp.abs(pre_up) < clamp_limit, grad_act * glu_part * sig_glu, 0.0
    ).astype(jnp.bfloat16)
    grad_down = jnp.einsum(
        "secf,secd->efd", activated, cot_in, preferred_element_type=jnp.float32
    ).astype(jnp.bfloat16)
    grad_gate = jnp.einsum(
        "secd,secf->edf", rows_in, grad_pre_gate, preferred_element_type=jnp.float32
    ).astype(jnp.bfloat16)
    grad_up = jnp.einsum(
        "secd,secf->edf", rows_in, grad_pre_up, preferred_element_type=jnp.float32
    ).astype(jnp.bfloat16)
    input_part = jnp.einsum(
        "secf,edf->secd", grad_pre_gate, w_gate, preferred_element_type=jnp.float32
    )
    input_part = input_part + jnp.einsum(
        "secf,edf->secd", grad_pre_up, w_up, preferred_element_type=jnp.float32
    )
    return (grad_gate, grad_up, grad_down, input_part)


def body(
    stream_in,
    out_cot,
    route_experts,
    route_weights,
    w_gate,
    w_up,
    w_down,
    w_proj,
    conv_value,
    conv_gate,
    conv_taps,
    conv_result,
    channel_norm_gain,
):
    sp_count = lax.axis_size("sp")
    tp_count = lax.axis_size("tp")
    local_experts = w_gate.shape[0]
    experts_all = local_experts * sp_count
    token_rows, model_width = stream_in.shape
    top_count = route_experts.shape[1]
    capacity = 2 * top_count * token_rows // experts_all
    slot_of, source_of = slot_tables(route_experts, experts_all, capacity)
    occupied = source_of >= 0
    source_safe = jnp.maximum(source_of, 0)
    token_of = source_safe // top_count
    slot_weight = jnp.where(occupied, route_weights.reshape(-1)[source_safe], 0.0)
    row_buffer = jnp.where(occupied[:, None], stream_in[token_of], jnp.zeros((), jnp.bfloat16))
    cot_buffer = (slot_weight[:, None] * out_cot[token_of].astype(jnp.float32)).astype(jnp.bfloat16)
    row_buffer = row_buffer.reshape(experts_all, capacity, model_width)
    cot_buffer = cot_buffer.reshape(experts_all, capacity, model_width)
    slice_width = model_width // tp_count
    slice_start = lax.axis_index("tp") * slice_width
    row_slice = lax.dynamic_slice_in_dim(row_buffer, slice_start, slice_width, 2)
    cot_slice = lax.dynamic_slice_in_dim(cot_buffer, slice_start, slice_width, 2)
    row_slice, cot_slice = (
        lax.all_to_all(row_slice, "sp", split_axis=0, concat_axis=0, tiled=True),
        lax.all_to_all(cot_slice, "sp", split_axis=0, concat_axis=0, tiled=True),
    )
    rows_in, cot_in = (
        lax.all_gather(row_slice, "tp", axis=2, tiled=True),
        lax.all_gather(cot_slice, "tp", axis=2, tiled=True),
    )
    rows_in = rows_in.reshape(sp_count, local_experts, capacity, model_width)
    cot_in = cot_in.reshape(sp_count, local_experts, capacity, model_width)
    grad_gate, grad_up, grad_down, input_part = expert_terms(rows_in, cot_in, w_gate, w_up, w_down)
    shared = lax.psum_scatter(
        input_part.astype(jnp.bfloat16), "tp", scatter_dimension=3, tiled=True
    )
    returned = shared.reshape(experts_all, capacity, slice_width)
    returned = lax.all_to_all(returned, "sp", split_axis=0, concat_axis=0, tiled=True)
    cot_cols = lax.dynamic_slice_in_dim(out_cot, slice_start, slice_width, 1)
    stream_part = combine_routes(returned, slot_of, cot_cols, token_rows, top_count)
    grad_stream = lax.all_gather(stream_part, "tp", axis=1, tiled=True)
    channel_total = conv_result.shape[0] * tp_count
    positions = conv_result.shape[1]
    conv_float = conv_result.astype(jnp.float32)
    chan_sum, chan_sq = lax.psum(
        (jnp.sum(conv_float, axis=0), jnp.sum(conv_float * conv_float, axis=0)), "tp"
    )
    chan_mean = chan_sum / channel_total
    chan_var = chan_sq / channel_total - chan_mean * chan_mean
    inverse_deviation = lax.rsqrt(chan_var + norm_eps)
    mean_removed = (conv_float - chan_mean) * inverse_deviation
    normalized_rows = mean_removed * channel_norm_gain[:, None]
    sigmoid_of_norm = jax.nn.sigmoid(normalized_rows)
    hidden = (normalized_rows * sigmoid_of_norm).astype(jnp.bfloat16)
    grad_proj = lax.psum_scatter(
        lax.dot_general(
            grad_stream, hidden, (((0,), (1,)), ((), ())), preferred_element_type=jnp.float32
        ),
        "sp",
        scatter_dimension=0,
        tiled=True,
    )
    hidden_gradient = lax.dot_general(
        w_proj, grad_stream, (((0,), (1,)), ((), ())), preferred_element_type=jnp.float32
    )
    normed_input_gradient = (
        hidden_gradient
        * sigmoid_of_norm
        * (1.0 + normalized_rows * (1.0 - sigmoid_of_norm))
        * channel_norm_gain[:, None]
    )
    average_products, cross_products = lax.psum(
        (
            jnp.sum(normed_input_gradient, axis=0),
            jnp.sum(normed_input_gradient * mean_removed, axis=0),
        ),
        "tp",
    )
    conv_output_gradient = inverse_deviation * (
        normed_input_gradient
        - average_products / channel_total
        - mean_removed * (cross_products / channel_total)
    )
    taps_count = conv_taps.shape[0]
    next_rim = from_behind(conv_output_gradient[:, : taps_count - 1], "sp", -1)
    extended = jnp.concatenate([conv_output_gradient, next_rim], axis=1)
    grad_gated = jnp.zeros_like(conv_output_gradient)
    for tap_index in range(taps_count):
        grad_gated = (
            grad_gated
            + conv_taps[tap_index][:, None] * extended[:, tap_index : tap_index + positions]
        )
    gate_sig = jax.nn.sigmoid(conv_gate.astype(jnp.float32))
    grad_value = (grad_gated * gate_sig).astype(jnp.bfloat16)
    grad_gate_in = (
        grad_gated * conv_value.astype(jnp.float32) * gate_sig * (1.0 - gate_sig)
    ).astype(jnp.bfloat16)
    return (grad_gate, grad_up, grad_down, grad_stream, grad_proj, grad_value, grad_gate_in)


def solution(mesh):
    return jax.shard_map(
        body,
        mesh=mesh,
        in_specs=(
            P("sp", None),
            P("sp", None),
            P("sp", None),
            P("sp", None),
            P("sp", None, "tp"),
            P("sp", None, "tp"),
            P("sp", "tp", None),
            P(None, "tp"),
            P("tp", "sp"),
            P("tp", "sp"),
            P(None, "tp"),
            P("tp", "sp"),
            P("tp"),
        ),
        out_specs=(
            P("sp", None, "tp"),
            P("sp", None, "tp"),
            P("sp", "tp", None),
            P("sp", None),
            P("sp", "tp"),
            P("tp", "sp"),
            P("tp", "sp"),
        ),
        check_vma=False,
    )
```

profile of v0, /device:TPU:0, one launch (start us, length us, event | category | flops | bytes accessed | tf_op | source)
XLA Modules:
  0.0 234.2 jit_solution(11183977361523465034)
XLA Ops:
  7.2 0.0 all-gather.3.cloned.1.call-start
  7.2 0.9 broadcast_multiply_fusion
  8.1 0.8 copy.26
  8.9 0.1 eq.29
  9.0 0.1 eq.25
  9.2 0.1 copy.25
  9.3 0.1 mul.442
  9.4 0.6 reduce-window.6
  10.0 0.2 slice_reduce_fusion
  10.3 0.1 fusion.150
  10.4 1.4 scatter_custom_fusion
  11.8 0.8 copy.28
  12.6 0.1 reshape.190
  12.8 3.5 %gather_fusion.1 = f32[512]{0:T(512)S(1)} fusion(f32[256]{0:T(256)S(1)} %reshape.190, s32[1024]{0:T(1024)S(1)} %get-tuple-element.71), kind=kCustom, calls=%fused_computation.1 | custom fusion | bytes 6144 | tf_op jit(solution)/shard_map/gather | solution.py:100
  16.3 0.1 broadcast_in_dim.46
  16.4 3.3 %gather_fusion = bf16[512,2048]{1,0:T(8,128)(2,1)} fusion(bf16[128,2048]{1,0:T(8,128)(2,1)S(1)} %copy-done.2, s32[1024]{0:T(1024)S(1)} %get-tuple-element.72), kind=kCustom, calls=%fused_computation | custom fusion | bytes 4196352 | tf_op jit(solution)/shard_map/gather | solution.py:101
  19.7 1.3 dynamic-slice_select_fusion
  21.0 21.7 %all_to_all.15 = bf16[8,64,512]{2,1,0:T(8,128)(2,1)} all-to-all(bf16[8,64,512]{2,1,0:T(8,128)(2,1)S(1)} %dynamic-slice_select_fusion), channel_id=1, replica_groups=mesh['sp'=8,'tp'=4] {'sp'}, dimensions={0} | all-to-all | bytes 1048576 | tf_op jit(solution)/shard_map/all_to_all | solution.py:110
  42.7 0.0 all-gather.3.cloned.1.call-update
  42.7 0.0 all-gather.5.cloned.1.call-start
  42.7 0.1 mul.445
  42.8 3.3 %gather_fusion.2 = bf16[512,2048]{1,0:T(8,128)(2,1)} fusion(bf16[128,2048]{1,0:T(8,128)(2,1)S(1)} %copy-done.1, s32[1024]{0:T(1024)S(1)} %get-tuple-element.72), kind=kCustom, calls=%fused_computation.2 | custom fusion | bytes 4196352 | tf_op jit(solution)/shard_map/gather | solution.py:102
  46.1 1.2 fusion.19
  47.3 17.6 %all_to_all.16 = bf16[8,64,512]{2,1,0:T(8,128)(2,1)} all-to-all(bf16[8,64,512]{2,1,0:T(8,128)(2,1)S(1)} %fusion.19), channel_id=1, replica_groups=mesh['sp'=8,'tp'=4] {'sp'}, dimensions={0} | all-to-all | bytes 1048576 | tf_op jit(solution)/shard_map/all_to_all | solution.py:111
  64.9 0.0 all-gather.5.cloned.1.call-update
  65.0 0.0 reduce-scatter.3.cloned.1.call-start
  65.0 0.0 all-gather.3.cloned.1.call-done
  65.0 4.6 %fusion.5 = f32[8,64,512]{2,1,0:T(8,128)} fusion(bf16[8,64,2048]{2,1,0:T(8,128)(2,1)} %all-gather.3.cloned.1.call-done, bf16[1,2048,512]{2,1,0:T(8,128)(2,1)} %param.18), kind=kOutput, calls=%fused_computation.14 | convolution fusion | flops 1073741824 | bytes 5242880 | tf_op jit(solution)/shard_map/secd,edf->secf/dot_general | solution.py:43
  69.6 2.2 fusion.11
  71.9 16.7 %all-gather.5.cloned.1.call-done = bf16[8,64,2048]{2,1,0:T(8,128)(2,1)} async-done(((bf16[8,64,512]{2,1,0:T(8,128)(2,1)}), bf16[8,64,2048]{2,1,0:T(8,128)(2,1)}) %all-gather.5.cloned.1.call-update) | async-done | bytes 2097168 | tf_op jit(solution)/shard_map/all_gather | solution.py:115
  88.6 4.7 %fusion.26 = (bf16[8,1,64,512]{3,2,0,1:T(8,128)(2,1)S(1)}, bf16[8,1,64,512]{3,2,0,1:T(8,128)(2,1)S(1)}) fusion(f32[8,64,512]{2,1,0:T(8,128)} %fusion.5, f32[8,64,512]{2,1,0:T(8,128)} %fusion.11, bf16[8,64,2048]{2,1,0:T(8,128)(2,1)} %all-gather.5.cloned.1.call-done, bf16[1,512,2048]{2,1,0:T(8,128)(2,1)} %param.19), kind=kOutput, calls=%fused_computation.69 | convolution fusion | flops 1079508992 | bytes 7340032 | tf_op jit(solution)/shard_map/secd,efd->secf/dot_general | solution.py:48
  93.3 1.3 fusion.9
  94.6 0.6 copy-done.3
  95.3 2.6 %fusion = bf16[8,1,64,2048]{3,2,0,1:T(8,128)(2,1)} fusion(f32[8,64,2048]{2,1,0:T(8,128)S(1)} %fusion.9, bf16[1,2048,512]{2,1,0:T(8,128)(2,1)S(1)} %copy-done.3, bf16[8,1,64,512]{3,2,0,1:T(8,128)(2,1)S(1)} %get-tuple-element.33), kind=kOutput, calls=%fused_computation.9 | convolution fusion | flops 1075838976 | bytes 8912896 | tf_op jit(solution)/shard_map/secf,edf->secd/dot_general | solution.py:68
  97.9 31.3 %reduce-scatter.3.cloned.1.call-done = bf16[8,1,64,512]{3,2,0,1:T(8,128)(2,1)} async-done(((bf16[8,1,64,2048]{3,2,0,1:T(8,128)(2,1)}), bf16[8,1,64,512]{3,2,0,1:T(8,128)(2,1)}) %reduce-scatter.3.cloned.1.call-update) | async-done | bytes 524304 | tf_op jit(solution)/shard_map/reduce_scatter | solution.py:120
  129.2 5.5 %all-to-all-start.2 = ((bf16[8,64,512]{2,1,0:T(8,128)(2,1)}), bf16[8,64,512]{2,1,0:T(8,128)(2,1)S(1)}, u32[]{:S(2)}, u32[]{:S(2)}) async-start(bf16[8,64,512]{2,1,0:T(8,128)(2,1)} %bitcast.190), calls=%async_computation.3 | async-start | bytes 1048576 | tf_op jit(solution)/shard_map/all_to_all | solution.py:124
  134.7 0.0 reduce-scatter.5.cloned.1.call-start
  134.8 0.1 copy.29
  134.9 0.1 convert_reduce_fusion
  135.0 6.1 %all-reduce.1 = (f32[128]{0:T(128)S(1)}, f32[128]{0:T(128)S(1)}) all-reduce(f32[128]{0:T(128)S(1)} %get-tuple-element.24, f32[128]{0:T(128)S(1)} %get-tuple-element.23), channel_id=1, replica_groups=mesh['sp'=8,'tp'=4] {'tp'}, use_global_device_ids=true, to_apply=%region_9.10 | all-reduce | flops 256 | bytes 2048 | tf_op jit(solution)/shard_map/psum | solution.py:131
  141.2 7.9 %all-to-all-done.2 = bf16[8,64,512]{2,1,0:T(8,128)(2,1)S(1)} async-done(((bf16[8,64,512]{2,1,0:T(8,128)(2,1)}), bf16[8,64,512]{2,1,0:T(8,128)(2,1)S(1)}, u32[]{:S(2)}, u32[]{:S(2)}) %all-to-all-start.2) | async-done | bytes 524320 | tf_op jit(solution)/shard_map/all_to_all | solution.py:124
  149.1 1.2 gather_fusion.3
  150.2 0.3 reshape.199
  150.6 0.6 reduce_sum.58
  151.2 6.5 %all_gather.11 = bf16[128,2048]{1,0:T(8,128)(2,1)S(1)} all-gather(bf16[128,512]{1,0:T(8,128)(2,1)S(1)} %add_convert_fusion.1), channel_id=1, replica_groups=mesh['sp'=8,'tp'=4] {'tp'}, dimensions={1}, use_global_device_ids=true | all-gather | bytes 655360 | tf_op jit(solution)/shard_map/all_gather | solution.py:127
  157.7 1.9 fusion.143
  159.7 0.1 copy.31
  159.8 0.1 copy.30
  159.9 0.6 fusion.162
  160.6 4.4 %fusion.1 = bf16[1,2048,512]{2,1,0:T(8,128)(2,1)} fusion(bf16[8,64,2048]{2,1,0:T(8,128)(2,1)} %all-gather.3.cloned.1.call-done, bf16[8,1,64,512]{3,2,0,1:T(8,128)(2,1)S(1)} %copy-done.7), kind=kOutput, calls=%fused_computation.10 | convolution fusion | flops 1074790400 | bytes 4718592 | tf_op jit(solution)/shard_map/secd,secf->edf/dot_general | solution.py:59
  165.0 2.8 %fusion.3 = bf16[1,512,2048]{2,1,0:T(8,128)(2,1)} fusion(bf16[8,64,2048]{2,1,0:T(8,128)(2,1)S(1)} %copy-done.28, f32[8,64,512]{2,1,0:T(8,128)S(1)} %copy-done.31, f32[8,64,512]{2,1,0:T(8,128)S(1)} %copy-done.30), kind=kOutput, calls=%fused_computation.12 | convolution fusion | flops 1077411840 | bytes 6291456 | tf_op jit(solution)/shard_map/secf,secd->efd/dot_general | solution.py:56
  167.8 0.9 fusion.160
  168.7 7.8 %all-reduce = (f32[128]{0:T(128)}, f32[128]{0:T(128)}) all-reduce(f32[128]{0:T(128)} %get-tuple-element.22, f32[128]{0:T(128)} %get-tuple-element.21), channel_id=1, replica_groups=mesh['sp'=8,'tp'=4] {'tp'}, use_global_device_ids=true, to_apply=%region_14.15 | all-reduce | flops 256 | bytes 2048 | tf_op jit(solution)/shard_map/psum | solution.py:158
  176.5 0.7 broadcast_multiply_fusion.1
  177.2 0.7 broadcast_multiply_fusion.2
  177.8 0.1 fusion.52
  178.1 1.3 collective-permute-start
  179.4 4.3 %fusion.2 = bf16[1,2048,512]{2,1,0:T(8,128)(2,1)} fusion(bf16[8,64,2048]{2,1,0:T(8,128)(2,1)} %all-gather.3.cloned.1.call-done, bf16[8,1,64,512]{3,2,0,1:T(8,128)(2,1)S(1)} %copy-done.5), kind=kOutput, calls=%fused_computation.11 | convolution fusion | flops 1074790400 | bytes 4718592 | tf_op jit(solution)/shard_map/secd,secf->edf/dot_general | solution.py:62
  183.7 0.2 collective-permute-done
  184.0 0.4 multiply_convert_fusion
  184.5 0.7 copy.32
  185.3 0.7 copy.33
  186.0 40.9 %reduce-scatter.5.cloned.1.call-done = f32[256,256]{1,0:T(8,128)} async-done(((f32[2048,256]{1,0:T(8,128)}), f32[256,256]{1,0:T(8,128)}) %reduce-scatter.5.cloned.1.call-update) | async-done | bytes 262160 | tf_op jit(solution)/shard_map/reduce_scatter | solution.py:141
  226.8 0.8 copy.35
  (79 shorter events, 0.4 us)
Async XLA Ops:
  7.2 62.5 %copy-start = (bf16[1,2048,512]{2,1,0:T(8,128)(2,1)S(1)}, bf16[1,2048,512]{2,1,0:T(8,128)(2,1)}, u32[]{:S(2)}) copy-start(bf16[1,2048,512]{2,1,0:T(8,128)(2,1)} %param.17) | copy-start | bytes 6291460
  7.2 9.2 %copy-start.2 = (bf16[128,2048]{1,0:T(8,128)(2,1)S(1)}, bf16[128,2048]{1,0:T(8,128)(2,1)}, u32[]{:S(2)}) copy-start(bf16[128,2048]{1,0:T(8,128)(2,1)} %param.13) | copy-start | bytes 1572868
  7.2 57.8 %all-gather.3.cloned.1.call-start = ((), (), s32[]{:S(2)}) async-start(), calls=%async_computation.5 | async-start | bytes 2621440 | tf_op jit(solution)/shard_map/all_gather | solution.py:114
  19.7 23.2 %copy-start.1 = (bf16[128,2048]{1,0:T(8,128)(2,1)S(1)}, bf16[128,2048]{1,0:T(8,128)(2,1)}, u32[]{:S(2)}) copy-start(bf16[128,2048]{1,0:T(8,128)(2,1)} %param.14) | copy-start | bytes 1572868
  42.7 45.9 %all-gather.5.cloned.1.call-start = ((), (), s32[]{:S(2)}) async-start(), calls=%async_computation.6 | async-start | bytes 2621440 | tf_op jit(solution)/shard_map/all_gather | solution.py:115
  65.0 64.3 %reduce-scatter.3.cloned.1.call-start = ((), (), s32[]{:S(2)}) async-start(), calls=%async_computation.7 | async-start | bytes 2621440 | tf_op jit(solution)/shard_map/reduce_scatter | solution.py:120
  65.0 4.6 %copy-start.27 = (bf16[8,64,2048]{2,1,0:T(8,128)(2,1)S(1)}, bf16[8,64,2048]{2,1,0:T(8,128)(2,1)}, u32[]{:S(2)}) copy-start(bf16[8,64,2048]{2,1,0:T(8,128)(2,1)} %all-gather.3.cloned.1.call-done) | copy-start | bytes 6291460
  93.3 1.4 copy-start.6
  93.3 1.3 copy-start.4
  93.3 2.0 copy-start.3
  97.9 36.9 %copy-start.8 = (bf16[256,128]{1,0:T(8,128)(2,1)S(1)}, bf16[256,128]{1,0:T(8,128)(2,1)}, u32[]{:S(2)}) copy-start(bf16[256,128]{1,0:T(8,128)(2,1)} %param.24) | copy-start | bytes 196612
  129.2 19.8 %all-to-all-start.2 = ((bf16[8,64,512]{2,1,0:T(8,128)(2,1)}), bf16[8,64,512]{2,1,0:T(8,128)(2,1)S(1)}, u32[]{:S(2)}, u32[]{:S(2)}) async-start(bf16[8,64,512]{2,1,0:T(8,128)(2,1)} %bitcast.190), calls=%async_computation.3 | async-start | bytes 1048576 | tf_op jit(solution)/shard_map/all_to_all | solution.py:124
  134.7 92.1 %reduce-scatter.5.cloned.1.call-start = ((), (), s32[]{:S(2)}) async-start(), calls=%async_computation.8 | async-start | bytes 2359296 | tf_op jit(solution)/shard_map/reduce_scatter | solution.py:141
  149.1 8.7 %copy-start.25 = (f32[256]{0:T(256)S(1)}, f32[256]{0:T(256)}, u32[]{:S(2)}) copy-start(f32[256]{0:T(256)} %param.25) | copy-start | bytes 3076
  157.7 1.9 copy-start.9
  157.7 2.0 copy-start.10
  157.7 2.2 copy-start.11
  157.7 2.8 %copy-start.7 = (bf16[8,1,64,512]{3,2,0,1:T(8,128)(2,1)S(1)}, bf16[8,1,64,512]{3,2,0,1:T(8,128)(2,1)}, u32[]{:S(2)}) copy-start(bf16[8,1,64,512]{3,2,0,1:T(8,128)(2,1)} %copy-done.6) | copy-start | bytes 1572868
  160.6 4.4 %copy-start.28 = (bf16[8,64,2048]{2,1,0:T(8,128)(2,1)S(1)}, bf16[8,64,2048]{2,1,0:T(8,128)(2,1)}, u32[]{:S(2)}) copy-start(bf16[8,64,2048]{2,1,0:T(8,128)(2,1)} %all-gather.5.cloned.1.call-done) | copy-start | bytes 6291460
  160.6 4.4 %copy-start.30 = (f32[8,64,512]{2,1,0:T(8,128)S(1)}, f32[8,64,512]{2,1,0:T(8,128)}, u32[]{:S(2)}) copy-start(f32[8,64,512]{2,1,0:T(8,128)} %fusion.5) | copy-start | bytes 3145732
  160.6 4.4 %copy-start.31 = (f32[8,64,512]{2,1,0:T(8,128)S(1)}, f32[8,64,512]{2,1,0:T(8,128)}, u32[]{:S(2)}) copy-start(f32[8,64,512]{2,1,0:T(8,128)} %fusion.11) | copy-start | bytes 3145732
  165.0 2.8 %copy-start.26 = (f32[256]{0:T(256)S(1)}, f32[256]{0:T(256)}, u32[]{:S(2)}) copy-start(f32[256]{0:T(256)} %param.25) | copy-start | bytes 3076
  165.0 2.8 %copy-start.29 = (bf16[2048,256]{1,0:T(8,128)(2,1)S(1)}, bf16[2048,256]{1,0:T(8,128)(2,1)}, u32[]{:S(2)}) copy-start(bf16[2048,256]{1,0:T(8,128)(2,1)} %param.20) | copy-start | bytes 3145732
  167.8 11.7 %copy-start.5 = (bf16[8,1,64,512]{3,2,0,1:T(8,128)(2,1)S(1)}, bf16[8,1,64,512]{3,2,0,1:T(8,128)(2,1)}, u32[]{:S(2)}) copy-start(bf16[8,1,64,512]{3,2,0,1:T(8,128)(2,1)} %copy-done.4) | copy-start | bytes 1572868
  178.0 5.9 %copy-start.12 = (f32[1,256]{1,0:T(1,128)S(1)}, f32[1,256]{1,0:T(1,128)}, u32[]{:S(2)}) copy-start(f32[1,256]{1,0:T(1,128)} %get-tuple-element.41) | copy-start | bytes 3076
  178.0 5.9 %copy-start.13 = (f32[1,256]{1,0:T(1,128)S(1)}, f32[1,256]{1,0:T(1,128)}, u32[]{:S(2)}) copy-start(f32[1,256]{1,0:T(1,128)} %get-tuple-element.42) | copy-start | bytes 3076
  178.0 5.9 %copy-start.14 = (f32[1,256]{1,0:T(1,128)S(1)}, f32[1,256]{1,0:T(1,128)}, u32[]{:S(2)}) copy-start(f32[1,256]{1,0:T(1,128)} %get-tuple-element.43) | copy-start | bytes 3076
  178.0 5.9 %copy-start.15 = (f32[1,256]{1,0:T(1,128)S(1)}, f32[1,256]{1,0:T(1,128)}, u32[]{:S(2)}) copy-start(f32[1,256]{1,0:T(1,128)} %get-tuple-element.44) | copy-start | bytes 3076
  178.0 5.9 %copy-start.16 = (f32[1,256]{1,0:T(1,128)S(1)}, f32[1,256]{1,0:T(1,128)}, u32[]{:S(2)}) copy-start(f32[1,256]{1,0:T(1,128)} %get-tuple-element.45) | copy-start | bytes 3076
  178.0 5.9 %copy-start.17 = (f32[1,256]{1,0:T(1,128)S(1)}, f32[1,256]{1,0:T(1,128)}, u32[]{:S(2)}) copy-start(f32[1,256]{1,0:T(1,128)} %get-tuple-element.46) | copy-start | bytes 3076
  178.1 5.9 %copy-start.18 = (f32[1,256]{1,0:T(1,128)S(1)}, f32[1,256]{1,0:T(1,128)}, u32[]{:S(2)}) copy-start(f32[1,256]{1,0:T(1,128)} %get-tuple-element.47) | copy-start | bytes 3076
  178.1 5.9 %copy-start.19 = (f32[1,256]{1,0:T(1,128)S(1)}, f32[1,256]{1,0:T(1,128)}, u32[]{:S(2)}) copy-start(f32[1,256]{1,0:T(1,128)} %get-tuple-element.48) | copy-start | bytes 3076
  178.1 5.9 %copy-start.20 = (f32[1,256]{1,0:T(1,128)S(1)}, f32[1,256]{1,0:T(1,128)}, u32[]{:S(2)}) copy-start(f32[1,256]{1,0:T(1,128)} %get-tuple-element.49) | copy-start | bytes 3076
  178.1 5.9 %copy-start.21 = (f32[1,256]{1,0:T(1,128)S(1)}, f32[1,256]{1,0:T(1,128)}, u32[]{:S(2)}) copy-start(f32[1,256]{1,0:T(1,128)} %get-tuple-element.50) | copy-start | bytes 3076
  178.1 5.9 %copy-start.22 = (f32[1,256]{1,0:T(1,128)S(1)}, f32[1,256]{1,0:T(1,128)}, u32[]{:S(2)}) copy-start(f32[1,256]{1,0:T(1,128)} %get-tuple-element.51) | copy-start | bytes 3076
  178.1 5.9 %copy-start.23 = (f32[1,256]{1,0:T(1,128)S(1)}, f32[1,256]{1,0:T(1,128)}, u32[]{:S(2)}) copy-start(f32[1,256]{1,0:T(1,128)} %get-tuple-element.52) | copy-start | bytes 3076
  178.1 5.9 %copy-start.24 = (f32[1,256]{1,0:T(1,128)S(1)}, f32[1,256]{1,0:T(1,128)}, u32[]{:S(2)}) copy-start(f32[1,256]{1,0:T(1,128)} %get-tuple-element.53) | copy-start | bytes 3076
  178.1 5.8 %collective-permute-start = (f32[256,30]{0,1:T(8,128)S(1)}, f32[256,30]{0,1:T(8,128)S(1)}, u32[]{:S(2)}, u32[]{:S(2)}) collective-permute-start(f32[256,30]{0,1:T(8,128)S(1)} %slice.265), channel_id=1, source_target_pairs={{4,0},{8,4},{12,8},{16,12},{20,16},{24,20},{28,24},{5,1},{9,5},{13... | collective-permute-start | bytes 92168 | tf_op jit(solution)/shard_map/ppermute | solution.py:14
Sparse Core Ops, SparseCore 0:
  42.8 21.5 all-gather.2
  66.0 22.5 all-gather.4
  98.0 31.1 reduce-scatter.2
  159.8 67.0 reduce-scatter.4
where the time goes:
time: 235 us; the launch traced here: 234 us
  waiting for transfers between devices  97.1 us (41%)
  blocking collectives  59.8 us (25%)
  matrix products  29.6 us (13%)
  local copies, waits for them, and re-layouts  19.6 us (8%)
  between operations  14.3 us (6%)
  starting transfers between devices  6.96 us (3%)
  other arithmetic  6.79 us (3%)
    reduce_scatter x1, waiting for transfers between devices, body(): lax.psum_scatter(lax.dot_general(grad_stream, hidden, (((0,), (1,)), ((),...  40.9 us
    reduce_scatter x1, waiting for transfers between devices, body(): lax.psum_scatter(input_part.astype(jnp.bfloat16), 'tp', scatter_dimension...  31.3 us
    all_to_all x1, blocking collectives, body(): lax.all_to_all(row_slice, 'sp', split_axis=0, concat_axis=0, tiled=True)  21.7 us
    all_to_all x1, blocking collectives, body(): lax.all_to_all(cot_slice, 'sp', split_axis=0, concat_axis=0, tiled=True)  17.6 us
    all_gather x1, waiting for transfers between devices, body(): lax.all_gather(cot_slice, 'tp', axis=2, tiled=True)  16.7 us
    all_to_all x1, waiting for transfers between devices, body(): lax.all_to_all(returned, 'sp', split_axis=0, concat_axis=0, tiled=True)  7.87 us
    psum x1, blocking collectives, body(): lax.psum((jnp.sum(normed_input_gradient, axis=0), jnp.sum(normed_input_gr...  7.82 us
    all_gather x1, blocking collectives, body(): grad_stream = lax.all_gather(stream_part, 'tp', axis=1, tiled=True)  6.5 us
  transfers between devices with their start and end apart: 6, of which 5 were waited for; matrix products, arithmetic and copies ran while one was open for 12% of the time, Pallas kernels for 0%

commit v1 on v0

--- a/solution.py
+++ b/solution.py
@@ -1,11 +1,479 @@
+import functools
+
 import jax
 import jax.numpy as jnp
 from jax import lax
+from jax.experimental import pallas as pl
+from jax.experimental.pallas import tpu as pltpu
 from jax.sharding import PartitionSpec as P
 
 norm_eps = 1e-05
 clamp_limit = 7.0
 alpha_gate = 1.702
+MESH = pl.DeviceIdType.MESH
+f32 = jnp.float32
+bf16 = jnp.bfloat16
+
+
+def dot(a, b, ca=1, cb=0):
+    return lax.dot_general(a, b, (((ca,), (cb,)), ((), ())), preferred_element_type=f32)
+
+
+def aligned(start, size):
+    return pl.ds(pl.multiple_of(start, size), size)
+
+
+def greet(n, s, q, tp_peers):
+    barrier = pltpu.get_barrier_semaphore()
+    for d in range(1, n):
+        pl.semaphore_signal(
+            barrier, inc=1, device_id={"sp": lax.rem(s + d, n), "tp": q}, device_id_type=MESH
+        )
+    for peer in tp_peers:
+        pl.semaphore_signal(barrier, inc=1, device_id={"sp": s, "tp": peer}, device_id_type=MESH)
+    pl.semaphore_wait(barrier, n - 1 + len(tp_peers))
+
+
+def remote(src, dst, send, recv, sp, tp):
+    return pltpu.make_async_remote_copy(
+        src_ref=src,
+        dst_ref=dst,
+        send_sem=send,
+        recv_sem=recv,
+        device_id={"sp": sp, "tp": tp},
+        device_id_type=MESH,
+    )
+
+
+def partners(q):
+    core, other = lax.rem(q, 2), q // 2
+    return (2 * other + 1 - core, 2 * (1 - other) + core, 2 * (1 - other) + 1 - core)
+
+
+def dispatch_kernel(
+    n, cap, routes_ref, weights_ref, stream_ref, cot_ref, rows_ref, cots_ref, pick_ref,
+    stage, send_xz, recv_xz, send_y, recv_y, send_c, recv_c, send_d, recv_d,
+):
+    s, q = lax.axis_index("sp"), lax.axis_index("tp")
+    q_core, q_y, q_far = partners(q)
+    top, tokens = routes_ref.shape
+    width = stage.shape[-1]
+    slots = pick_ref.shape[0]
+    experts = slots // cap
+
+    greet(n, s, q, (q_core, q_y))
+
+    routes = routes_ref[...]
+    expert_ids = lax.broadcasted_iota(jnp.int32, (experts, tokens), 0)
+    hits = [expert_ids == routes[k : k + 1, :] for k in range(top)]
+    count = sum(h.astype(f32) for h in hits)
+    earlier = (
+        lax.broadcasted_iota(jnp.int32, (tokens, tokens), 0)
+        < lax.broadcasted_iota(jnp.int32, (tokens, tokens), 1)
+    ).astype(f32)
+    before = dot(count.astype(bf16), earlier.astype(bf16))
+    slot_ids = lax.broadcasted_iota(jnp.int32, (slots, tokens), 0)
+    pick = jnp.zeros((slots, tokens), f32)
+    weighted = jnp.zeros((slots, tokens), f32)
+    for k in range(top):
+        rank = jnp.sum(jnp.where(hits[k], before, 0.0), axis=0, keepdims=True)
+        slot = routes[k : k + 1, :] * cap + rank.astype(jnp.int32)
+        here = slot_ids == slot
+        pick = jnp.where(here, 1.0, pick)
+        weighted = jnp.where(here, weights_ref[k : k + 1, :], weighted)
+    slot_weight = jnp.sum(weighted, axis=1, keepdims=True)
+    pick = pick.astype(bf16)
+    pick_ref[...] = pick
+    own = aligned(q * width, width)
+    picked = dot(pick, stream_ref[:, own]).astype(bf16)
+    stage[0] = picked
+    stage[1] = (slot_weight * dot(pick, cot_ref[:, own])).astype(bf16)
+
+    outs = (rows_ref, cots_ref)
+    copies = []
+
+    def start(copy):
+        copy.start()
+        copies.append(copy)
+        return copy
+
+    def at(a, source, quarter):
+        return outs[a].at[aligned(source * cap, cap), aligned(quarter * width, width)]
+
+    arriving = []
+    for d in range(1, n):
+        dest = lax.rem(s + d, n)
+        arriving.append(
+            [
+                start(
+                    remote(
+                        stage.at[a, aligned(dest * cap, cap)], at(a, s, q),
+                        send_xz.at[a, d], recv_xz.at[a, d], dest, q,
+                    )
+                )
+                for a in range(2)
+            ]
+        )
+    for a in range(2):
+        outs[a][aligned(s * cap, cap), own] = stage[a, aligned(s * cap, cap), :]
+
+    across, tail = [], []
+
+    def far_forward(d):
+        source = lax.rem(s + n - d, n)
+        for a in range(2):
+            across[d][a].wait_recv()
+            tail.append(
+                start(
+                    remote(
+                        at(a, source, q_y), at(a, source, q_y),
+                        send_d.at[a, d], recv_d.at[a, d], s, q_core,
+                    )
+                )
+            )
+
+    for d in range(n):
+        source = lax.rem(s + n - d, n)
+        row = []
+        for a in range(2):
+            if d > 0:
+                arriving[d - 1][a].wait_recv()
+            block = at(a, source, q)
+            row.append(start(remote(block, block, send_y.at[a, d], recv_y.at[a, d], s, q_y)))
+            tail.append(start(remote(block, block, send_c.at[a, d], recv_c.at[a, d], s, q_core)))
+        across.append(row)
+        if d > 0:
+            far_forward(d - 1)
+    far_forward(n - 1)
+    for copy in tail:
+        copy.wait_recv()
+    for copy in copies:
+        copy.wait_send()
+
+
+def dispatch(stream_in, out_cot, routes, weights, n, cap, tp_count, experts):
+    tokens, model_width = stream_in.shape
+    width = model_width // tp_count
+    slots = experts * cap
+    dma = [pltpu.SemaphoreType.DMA((2, n))] * 8
+    return pl.pallas_call(
+        functools.partial(dispatch_kernel, n, cap),
+        out_shape=(
+            jax.ShapeDtypeStruct((n * cap, model_width), bf16),
+            jax.ShapeDtypeStruct((n * cap, model_width), bf16),
+            jax.ShapeDtypeStruct((slots, tokens), bf16),
+        ),
+        in_specs=[pl.BlockSpec(memory_space=pltpu.VMEM)] * 4,
+        out_specs=[pl.BlockSpec(memory_space=pltpu.VMEM)] * 3,
+        scratch_shapes=[pltpu.VMEM((2, slots, width), bf16)] + dma,
+        compiler_params=pltpu.CompilerParams(
+            collective_id=0, has_side_effects=True, vmem_limit_bytes=24 << 20
+        ),
+        name="dispatch",
+    )(routes, weights, stream_in, out_cot)
+
+
+def tail_kernel(
+    n, cap, channel_total,
+    part_ref, pick_ref, cot_ref, proj_ref, value_ref, gate_ref, taps_ref, conv_ref, gain_ref,
+    gs_ref, gproj_ref, gvalue_ref, ggate_ref,
+    from_core, own, to_y, from_y, to_xz, ret, hid_all, col_all, stat, stat2, ext,
+    send_c, recv_c, send_y, recv_y, send_r, recv_r, send_h, recv_h, send_s, recv_s,
+    send_g, recv_g, send_k, recv_k, send_f, recv_f, send_e, recv_e,
+):
+    s, q = lax.axis_index("sp"), lax.axis_index("tp")
+    q_core, q_y, q_far = partners(q)
+    peers = (q_core, q_y, q_far)
+    core, y = lax.rem(q, 2), q // 2
+    tokens, model_width = gs_ref.shape
+    width = ret.shape[-1]
+    icols = gproj_ref.shape[0]
+    taps_count = taps_ref.shape[0]
+    copies = []
+
+    def start(copy):
+        copy.start()
+        copies.append(copy)
+        return copy
+
+    greet(n, s, q, peers)
+
+    order = [lax.rem(s + d, n) for d in range(1, n)] + [s]
+    from_c = []
+    for j, b in enumerate(order):
+        rows = aligned(b * cap, cap)
+        from_c.append(
+            [
+                start(
+                    remote(
+                        part_ref.at[rows, aligned((2 * half + 1 - core) * width, width)],
+                        from_core.at[h, rows],
+                        send_c.at[h, j], recv_c.at[h, j], s, q_core,
+                    )
+                )
+                for h, half in ((0, 1 - y), (1, y))
+            ]
+        )
+
+    def exchange_stats(buffer, first, second, which):
+        lanes = lax.broadcasted_iota(jnp.int32, (tokens, tokens), 1)
+        packed = jnp.where(lanes == 0, first, jnp.where(lanes == 1, second, 0.0))
+        buffer[3] = packed.T[0:8, :]
+        return [
+            start(
+                remote(
+                    buffer.at[3], buffer.at[p], send_s.at[which, p], recv_s.at[which, p], s, peer
+                )
+            )
+            for p, peer in enumerate(peers)
+        ]
+
+    def summed_stats(buffer, waits):
+        for w in waits:
+            w.wait_recv()
+        total = (buffer[3] + buffer[0]) + (buffer[1] + buffer[2])
+        wide = jnp.concatenate([total, jnp.zeros((tokens - 8, tokens), f32)], axis=0).T
+        return wide[:, 0:1], wide[:, 1:2]
+
+    conv = conv_ref[...].astype(f32).T
+    stat_waits = exchange_stats(
+        stat,
+        jnp.sum(conv, axis=1, keepdims=True),
+        jnp.sum(conv * conv, axis=1, keepdims=True),
+        0,
+    )
+    over_y = []
+    for j, b in enumerate(order):
+        rows = aligned(b * cap, cap)
+        from_c[j][0].wait_recv()
+        to_y[rows, :] = (
+            part_ref[rows, aligned((2 * (1 - y) + core) * width, width)].astype(f32)
+            + from_core[0, rows, :].astype(f32)
+        ).astype(bf16)
+        over_y.append(
+            start(
+                remote(to_y.at[rows], from_y.at[rows], send_y.at[j], recv_y.at[j], s, q_y)
+            )
+        )
+    for j, b in enumerate(order):
+        rows = aligned(b * cap, cap)
+        from_c[j][1].wait_recv()
+        own[rows, :] = part_ref[rows, aligned(q * width, width)].astype(f32) + from_core[
+            1, rows, :
+        ].astype(f32)
+    chan_sum, chan_sq = summed_stats(stat, stat_waits)
+    chan_mean = chan_sum / channel_total
+    chan_var = chan_sq / channel_total - chan_mean * chan_mean
+    inverse_deviation = lax.rsqrt(chan_var + norm_eps)
+    mean_removed = (conv - chan_mean) * inverse_deviation
+    gain = gain_ref[...]
+    normed = mean_removed * gain
+    sig = jax.nn.sigmoid(normed)
+    hid_all[aligned(s * tokens, tokens), :] = (normed * sig).astype(bf16)
+    slope = sig * (1.0 + normed * (1.0 - sig)) * gain
+    back = []
+    for j, b in enumerate(order):
+        rows = aligned(b * cap, cap)
+        over_y[j].wait_recv()
+        total = (own[rows, :] + from_y[rows, :].astype(f32)).astype(bf16)
+        if j == n - 1:
+            ret[rows, :] = total
+        else:
+            to_xz[rows, :] = total
+            back.append(
+                start(
+                    remote(
+                        to_xz.at[rows], ret.at[aligned(s * cap, cap)],
+                        send_r.at[j], recv_r.at[j], b, q,
+                    )
+                )
+            )
+    mine = aligned(s * tokens, tokens)
+    hid_waits = [
+        start(
+            remote(hid_all.at[mine], hid_all.at[mine], send_h.at[j], recv_h.at[j], order[j], q)
+        )
+        for j in range(n - 1)
+    ]
+    for copy in back:
+        copy.wait_recv()
+    quarter = aligned(q * width, width)
+    combined = dot(pick_ref[...], ret[...], 0, 0) + cot_ref[:, quarter].astype(f32)
+    gs_ref[:, quarter] = combined.astype(bf16)
+    quarter_y = aligned(q_y * width, width)
+    by_core = start(
+        remote(gs_ref.at[:, quarter], gs_ref.at[:, quarter], send_g.at[0], recv_g.at[0], s, q_core)
+    )
+    by_y = start(
+        remote(gs_ref.at[:, quarter], gs_ref.at[:, quarter], send_g.at[1], recv_g.at[1], s, q_y)
+    )
+
+    def partial_of(owner):
+        cols = aligned(owner * width, width)
+        return dot(gs_ref[:, cols], proj_ref[cols, :])
+
+    grad_hidden = partial_of(q)
+    by_y.wait_recv()
+    by_far = start(
+        remote(
+            gs_ref.at[:, quarter_y], gs_ref.at[:, quarter_y], send_g.at[2], recv_g.at[2], s, q_core
+        )
+    )
+    grad_hidden = grad_hidden + partial_of(q_y)
+    by_core.wait_recv()
+    grad_hidden = grad_hidden + partial_of(q_core)
+    by_far.wait_recv()
+    grad_hidden = grad_hidden + partial_of(q_far)
+    half_rows = tokens // 2
+    part_rows = aligned(core * half_rows, half_rows)
+    land = aligned(s * tokens + core * half_rows, half_rows)
+    col_waits = [
+        start(
+            remote(
+                gs_ref.at[part_rows, aligned(order[j] * icols, icols)], col_all.at[land],
+                send_k.at[j], recv_k.at[j], order[j], q,
+            )
+        )
+        for j in range(n - 1)
+    ]
+    col_all[mine, :] = gs_ref[:, aligned(s * icols, icols)]
+    norm_grad = grad_hidden * slope
+    stat_waits = exchange_stats(
+        stat2,
+        jnp.sum(norm_grad, axis=1, keepdims=True),
+        jnp.sum(norm_grad * mean_removed, axis=1, keepdims=True),
+        1,
+    )
+    avg, cross = summed_stats(stat2, stat_waits)
+    conv_grad = inverse_deviation * (
+        norm_grad - avg / channel_total - mean_removed * (cross / channel_total)
+    )
+    rim = ext.shape[0] - tokens
+    ext[0:tokens, :] = conv_grad
+    halo = start(
+        remote(
+            ext.at[0:rim], ext.at[tokens : tokens + rim], send_e.at[0], recv_e.at[0],
+            lax.rem(s + n - 1, n), q,
+        )
+    )
+    forwards = []
+    for j in range(n - 1):
+        col_waits[j].wait_recv()
+        source = lax.rem(s + n - (j + 1), n)
+        there = aligned(source * tokens + core * half_rows, half_rows)
+        forwards.append(
+            start(
+                remote(col_all.at[there], col_all.at[there], send_f.at[j], recv_f.at[j], s, q_core)
+            )
+        )
+    halo.wait_recv()
+    edge = ext[tokens : tokens + rim, :]
+    halo.wait_send()
+    ext[tokens : tokens + rim, :] = jnp.where(s == n - 1, 0.0, edge)
+    acc = jnp.zeros((tokens, ext.shape[1]), f32)
+    for tap in range(taps_count):
+        acc = acc + taps_ref[tap : tap + 1, :] * ext[tap : tap + tokens, :]
+    gated = acc.T
+    gate_sig = jax.nn.sigmoid(gate_ref[...].astype(f32))
+    gvalue_ref[...] = (gated * gate_sig).astype(bf16)
+    ggate_ref[...] = (
+        gated * value_ref[...].astype(f32) * gate_sig * (1.0 - gate_sig)
+    ).astype(bf16)
+    for copy in hid_waits + forwards:
+        copy.wait_recv()
+    gproj_ref[...] = dot(col_all[...], hid_all[...], 0, 0)
+    for copy in copies:
+        if copy is not halo:
+            copy.wait_send()
+
+
+def tail(part, pick, out_cot, w_proj, value, gate, taps, conv, gain, n, cap, tp_count):
+    tokens, model_width = out_cot.shape
+    width = model_width // tp_count
+    channels = value.shape[0]
+    icols = model_width // n
+    slots = pick.shape[0]
+    rows = part.shape[0]
+    rim = -(-(taps.shape[0] - 1) // 8) * 8
+    V = pltpu.VMEM
+    dma = pltpu.SemaphoreType.DMA
+    pairs = [(2, n), (n,), (n,), (n,), (2, 3), (3,), (n,), (n,), (1,)]
+    return pl.pallas_call(
+        functools.partial(tail_kernel, n, cap, channels * tp_count),
+        out_shape=(
+            jax.ShapeDtypeStruct((tokens, model_width), bf16),
+            jax.ShapeDtypeStruct((icols, channels), f32),
+            jax.ShapeDtypeStruct((channels, tokens), bf16),
+            jax.ShapeDtypeStruct((channels, tokens), bf16),
+        ),
+        in_specs=[pl.BlockSpec(memory_space=V)] * 9,
+        out_specs=[pl.BlockSpec(memory_space=V)] * 4,
+        scratch_shapes=[
+            V((2, rows, width), bf16),
+            V((rows, width), f32),
+            V((rows, width), bf16),
+            V((rows, width), bf16),
+            V((rows, width), bf16),
+            V((slots, width), bf16),
+            V((n * tokens, channels), bf16),
+            V((n * tokens, icols), bf16),
+            V((4, 8, tokens), f32),
+            V((4, 8, tokens), f32),
+            V((tokens + rim, channels), f32),
+        ]
+        + [dma(shape) for shape in pairs for _ in range(2)],
+        compiler_params=pltpu.CompilerParams(
+            collective_id=1, has_side_effects=True, vmem_limit_bytes=40 << 20
+        ),
+        name="combine_tail",
+    )(part, pick, out_cot, w_proj, value, gate, taps, conv, gain)
+
+
+def expert_terms(rows_in, cot_in, w_gate, w_up, w_down):
+    pre_gate = dot(rows_in, w_gate)
+    pre_up = dot(rows_in, w_up)
+    glu_part = jnp.minimum(pre_gate, clamp_limit)
+    lin_part = jnp.clip(pre_up, -clamp_limit, clamp_limit)
+    sig_glu = jax.nn.sigmoid(alpha_gate * glu_part)
+    activated = (glu_part * sig_glu * (lin_part + 1.0)).astype(bf16)
+    grad_act = dot(cot_in, w_down, 1, 1)
+    slope = sig_glu + alpha_gate * glu_part * sig_glu * (1.0 - sig_glu)
+    grad_pre_gate = jnp.where(
+        pre_gate < clamp_limit, grad_act * (lin_part + 1.0) * slope, 0.0
+    ).astype(bf16)
+    grad_pre_up = jnp.where(
+        jnp.abs(pre_up) < clamp_limit, grad_act * glu_part * sig_glu, 0.0
+    ).astype(bf16)
+    grad_down = dot(activated, cot_in, 0, 0).astype(bf16)
+    grad_gate = dot(rows_in, grad_pre_gate, 0, 0).astype(bf16)
+    grad_up = dot(rows_in, grad_pre_up, 0, 0).astype(bf16)
+    input_part = dot(grad_pre_gate, w_gate, 1, 1) + dot(grad_pre_up, w_up, 1, 1)
+    return (grad_gate, grad_up, grad_down, input_part.astype(bf16))
+
+
+def body(
+    stream_in, out_cot, route_experts, route_weights, w_gate, w_up, w_down, w_proj,
+    conv_value, conv_gate, conv_taps, conv_result, channel_norm_gain,
+):
+    n = lax.axis_size("sp")
+    tp_count = lax.axis_size("tp")
+    experts = w_gate.shape[0] * n
+    tokens, model_width = stream_in.shape
+    cap = 2 * route_experts.shape[1] * tokens // experts
+    rows_in, cot_in, pick = dispatch(
+        stream_in, out_cot, route_experts.T, route_weights.T, n, cap, tp_count, experts
+    )
+    grad_gate, grad_up, grad_down, part = expert_terms(
+        rows_in, cot_in, w_gate[0], w_up[0], w_down[0]
+    )
+    grad_stream, grad_proj, grad_value, grad_gate_in = tail(
+        part, pick, out_cot, w_proj, conv_value, conv_gate, conv_taps, conv_result,
+        channel_norm_gain[None, :], n, cap, tp_count,
+    )
+    return (
+        grad_gate[None], grad_up[None], grad_down[None],
+        grad_stream, grad_proj, grad_value, grad_gate_in,
+    )
 
 
 def from_behind(value, axis, steps):
@@ -38,7 +506,7 @@
     return (cot_cols.astype(jnp.float32) + jnp.sum(per_route, axis=1)).astype(jnp.bfloat16)
 
 
-def expert_terms(rows_in, cot_in, w_gate, w_up, w_down):
+def expert_terms_plain(rows_in, cot_in, w_gate, w_up, w_down):
     pre_gate = jnp.einsum("secd,edf->secf", rows_in, w_gate, preferred_element_type=jnp.float32)
     pre_up = jnp.einsum("secd,edf->secf", rows_in, w_up, preferred_element_type=jnp.float32)
     glu_part = jnp.minimum(pre_gate, clamp_limit)
@@ -71,7 +539,7 @@
     return (grad_gate, grad_up, grad_down, input_part)
 
 
-def body(
+def body_plain(
     stream_in,
     out_cot,
     route_experts,
@@ -116,7 +584,7 @@
     )
     rows_in = rows_in.reshape(sp_count, local_experts, capacity, model_width)
     cot_in = cot_in.reshape(sp_count, local_experts, capacity, model_width)
-    grad_gate, grad_up, grad_down, input_part = expert_terms(rows_in, cot_in, w_gate, w_up, w_down)
+    grad_gate, grad_up, grad_down, input_part = expert_terms_plain(rows_in, cot_in, w_gate, w_up, w_down)
     shared = lax.psum_scatter(
         input_part.astype(jnp.bfloat16), "tp", scatter_dimension=3, tiled=True
     )
@@ -186,7 +654,7 @@
 
 def solution(mesh):
     return jax.shard_map(
-        body,
+        body if mesh.shape["tp"] == 4 else body_plain,
         mesh=mesh,
         in_specs=(
             P("sp", None),

time: 235 us -> 109 us (0.46)
  waiting for transfers between devices: 97.1 us -> 0 us
  Pallas kernels: 0 us -> 84 us
  blocking collectives: 59.8 us -> 0 us
  between operations: 14.3 us -> 0.77 us
  matrix products: 29.6 us -> 16.6 us
  local copies, waits for them, and re-layouts: 19.6 us -> 7.03 us
  starting transfers between devices: 6.96 us -> 0 us
  other arithmetic: 6.79 us -> 0 us
    pallas_call x0 -> x2, Pallas kernels: none -> 84 us  [the longest x1 44.9 us: tail(): pl.pallas_call(functools.partial(tail_kernel, n, cap, channels * tp_count...]
    reduce_scatter x2 -> x0, waiting for transfers between devices: 72.2 us -> none  [the longest x1 40.9 us: body(): lax.psum_scatter(lax.dot_general(grad_stream, hidden, (((0,), (1,)), ((),...]
    all_to_all x2 -> x0, blocking collectives: 39.3 us -> none  [the longest x1 21.7 us: body(): lax.all_to_all(row_slice, 'sp', split_axis=0, concat_axis=0, tiled=True)]
    all_gather x2 -> x0, waiting for transfers between devices: 16.7 us -> none  [the longest x1 16.7 us: body(): lax.all_gather(cot_slice, 'tp', axis=2, tiled=True)]
    psum x2 -> x0, blocking collectives: 14 us -> none  [the longest x1 7.82 us: body(): lax.psum((jnp.sum(normed_input_gradient, axis=0), jnp.sum(normed_input_gr...]
    dot_general x10 -> x8, matrix products: 29.6 us -> 16.6 us  [dot(): lax.dot_general(a, b, (((ca,), (cb,)), ((), ())), preferred_element_type=...]
    gather x4 -> x0, local copies, waits for them, and re-layouts: 11.2 us -> none  [the longest x1 3.51 us: body(): route_weights.reshape(-1)[source_safe]]
    all_to_all x1 -> x0, waiting for transfers between devices: 7.87 us -> none  [body(): lax.all_to_all(returned, 'sp', split_axis=0, concat_axis=0, tiled=True)]
  transfers between devices with their start and end apart: 6 -> 0, of which waited for: 5 -> 0; matrix products, arithmetic and copies ran while one was open for 12% -> 0% of each run, Pallas kernels for 0% -> 0%
where the time goes in v1:
time: 109 us; the launch traced here: 108 us
  Pallas kernels  84 us (77%)
  matrix products  16.6 us (15%)
  local copies, waits for them, and re-layouts  7.03 us (6%)
    pallas_call x1, Pallas kernels, tail(): pl.pallas_call(functools.partial(tail_kernel, n, cap, channels * tp_count...  44.9 us
    pallas_call x1, Pallas kernels, dispatch(): pl.pallas_call(functools.partial(dispatch_kernel, n, cap), out_shape=(jax...  39.1 us
    dot_general x8, matrix products, dot(): lax.dot_general(a, b, (((ca,), (cb,)), ((), ())), preferred_element_type=...  16.6 us
    unnamed x32, local copies, waits for them, and re-layouts  7.03 us

profile of v1, /device:TPU:0, one launch (start us, length us, event | category | flops | bytes accessed | tf_op | source)
XLA Modules:
  0.0 108.4 jit_solution(10502767693266931623)
XLA Ops:
  0.6 0.0 copy-start
  0.6 0.0 copy-start.1
  0.7 1.2 %copy-done.1 = bf16[128,2048]{1,0:T(8,128)(2,1)S(1)} copy-done((bf16[128,2048]{1,0:T(8,128)(2,1)S(1)}, bf16[128,2048]{1,0:T(8,128)(2,1)}, u32[]{:S(2)}) %copy-start.1) | copy-done | bytes 524312
  1.8 0.0 copy-start.4
  1.8 1.0 copy-done.4
  2.9 0.0 copy-start.10
  2.9 0.7 copy-done.10
  3.6 0.0 copy-start.11
  3.6 0.7 copy-done.11
  4.2 39.1 %dispatch.1 = (bf16[512,2048]{1,0:T(8,128)(2,1)S(1)}, bf16[512,2048]{1,0:T(8,128)(2,1)S(1)}, bf16[512,128]{1,0:T(8,128)(2,1)S(1)}) custom-call(s32[2,128]{1,0:T(2,128)S(1)} %bitcast.35, f32[2,128]{1,0:T(2,128)S(1)} %bitcast.36, bf16[128,2048]{1,0:T(8,128)(2,1)S(1)} %copy-done.4, bf16[128,2048]{1,0:T(8,128)(2,1)S(1)} %copy-done.1), custom_call_target="tpu_custom_call" | custom-call | tf_op jit(solution)/shard_map/dispatch/pallas_call | solution.py:159
  43.3 2.8 %fusion.4 = f32[512,512]{1,0:T(8,128)S(1)} fusion(bf16[512,2048]{1,0:T(8,128)(2,1)S(1)} %get-tuple-element.14, bf16[1,2048,512]{2,1,0:T(8,128)(2,1)} %param.18), kind=kOutput, calls=%fused_computation.8 | convolution fusion | flops 1073741824 | bytes 5242880 | tf_op jit(solution)/shard_map/dot_general | solution.py:19
  46.2 0.0 copy-done
  46.2 0.0 copy-start.13
  46.2 1.3 %fusion.10 = f32[512,512]{1,0:T(8,128)S(1)} fusion(bf16[512,2048]{1,0:T(8,128)(2,1)S(1)} %get-tuple-element.14, bf16[1,2048,512]{2,1,0:T(8,128)(2,1)S(1)} %copy-done), kind=kOutput, calls=%fused_computation.14 | convolution fusion | flops 1073741824 | bytes 5242880 | tf_op jit(solution)/shard_map/dot_general | solution.py:19
  47.5 0.3 copy-done.13
  47.8 1.9 %select_convert_fusion = (bf16[512,512]{1,0:T(8,128)(2,1)S(1)}, bf16[512,512]{1,0:T(8,128)(2,1)S(1)}) fusion(f32[512,512]{1,0:T(8,128)S(1)} %fusion.4, f32[512,512]{1,0:T(8,128)S(1)} %fusion.10, bf16[512,2048]{1,0:T(8,128)(2,1)S(1)} %get-tuple-element.15, bf16[1,512,2048]{2,1,0:T(8,128)(2,1)S(1)} %copy-done.13), kind=kOutput, calls=%fused_computation.17 | convolution fusion | flops 1079508992 | bytes 7340032 | tf_op jit(solution)/shard_map/dot_general | solution.py:19
  49.7 2.8 %fusion.2 = bf16[1,512,2048]{2,1,0:T(8,128)(2,1)} fusion(bf16[512,2048]{1,0:T(8,128)(2,1)S(1)} %get-tuple-element.15, f32[512,512]{1,0:T(8,128)S(1)} %fusion.10, f32[512,512]{1,0:T(8,128)S(1)} %fusion.4), kind=kOutput, calls=%fused_computation.6 | convolution fusion | flops 1077411840 | bytes 6291456 | tf_op jit(solution)/shard_map/dot_general | solution.py:19
  52.5 2.6 %fusion.1 = bf16[1,2048,512]{2,1,0:T(8,128)(2,1)} fusion(bf16[512,2048]{1,0:T(8,128)(2,1)S(1)} %get-tuple-element.14, bf16[512,512]{1,0:T(8,128)(2,1)S(1)} %get-tuple-element.21), kind=kOutput, calls=%fused_computation.5 | convolution fusion | flops 1074790400 | bytes 4718592 | tf_op jit(solution)/shard_map/dot_general | solution.py:19
  55.1 2.6 %fusion = bf16[1,2048,512]{2,1,0:T(8,128)(2,1)} fusion(bf16[512,2048]{1,0:T(8,128)(2,1)S(1)} %get-tuple-element.14, bf16[512,512]{1,0:T(8,128)(2,1)S(1)} %get-tuple-element.22), kind=kOutput, calls=%fused_computation.4 | convolution fusion | flops 1074790400 | bytes 4718592 | tf_op jit(solution)/shard_map/dot_general | solution.py:19
  57.8 0.0 copy-start.12
  57.8 1.3 %fusion.8 = f32[512,2048]{1,0:T(8,128)S(1)} fusion(bf16[512,512]{1,0:T(8,128)(2,1)S(1)} %get-tuple-element.22, bf16[1,2048,512]{2,1,0:T(8,128)(2,1)S(1)} %copy-done), kind=kOutput, calls=%fused_computation.12 | convolution fusion | flops 1073741824 | bytes 6815744 | tf_op jit(solution)/shard_map/dot_general | solution.py:19
  59.1 0.3 copy-done.12
  59.3 0.0 copy-start.2
  59.3 0.0 copy-start.3
  59.3 0.0 copy-start.5
  59.4 0.0 copy-start.6
  59.4 0.0 copy-start.7
  59.4 0.0 copy-start.8
  59.4 0.0 copy-start.9
  59.4 1.3 %add_convert_fusion.part_ref = bf16[512,2048]{1,0:T(8,128)(2,1)S(1)} fusion(f32[512,2048]{1,0:T(8,128)S(1)} %fusion.8, bf16[512,512]{1,0:T(8,128)(2,1)S(1)} %get-tuple-element.21, bf16[1,2048,512]{2,1,0:T(8,128)(2,1)S(1)} %copy-done.12), kind=kOutput, calls=%fused_computation | convolution fusion | flops 1075838976 | bytes 8912896 | tf_op jit(solution)/shard_map/dot_general | solution.py:19
  60.7 0.0 copy-done.2
  60.7 0.0 copy-done.3
  60.7 0.0 copy-done.5
  60.7 0.0 copy-done.6
  60.7 0.0 copy-done.7
  60.7 0.0 copy-done.8
  60.7 0.0 copy-done.9
  60.8 44.9 %combine_tail.1 = (bf16[128,2048]{1,0:T(8,128)(2,1)S(1)}, f32[256,256]{1,0:T(8,128)S(1)}, bf16[256,128]{1,0:T(8,128)(2,1)S(1)}, bf16[256,128]{1,0:T(8,128)(2,1)S(1)}) custom-call(bf16[512,2048]{1,0:T(8,128)(2,1)S(1)} %add_convert_fusion.part_ref, bf16[512,128]{1,0:T(8,128)(2,1)S(1)} %get-tuple-element.16.pick_ref, bf16[128,2048]{1,0:T(8,128)(2,1)S(1)} %copy-done.2, ...), custom_call_target="tpu_custom_call" | custom-call | tf_op jit(solution)/shard_map/combine_tail/pallas_call | solution.py:401
  105.7 0.8 copy.24
  106.5 0.7 copy.25
  107.2 0.6 copy.26
  107.8 0.6 copy.27
Async XLA Ops:
  0.6 45.6 %copy-start = (bf16[1,2048,512]{2,1,0:T(8,128)(2,1)S(1)}, bf16[1,2048,512]{2,1,0:T(8,128)(2,1)}, u32[]{:S(2)}) copy-start(bf16[1,2048,512]{2,1,0:T(8,128)(2,1)} %param.17) | copy-start | bytes 6291460
  0.6 1.2 %copy-start.1 = (bf16[128,2048]{1,0:T(8,128)(2,1)S(1)}, bf16[128,2048]{1,0:T(8,128)(2,1)}, u32[]{:S(2)}) copy-start(bf16[128,2048]{1,0:T(8,128)(2,1)} %cot_ref.3) | copy-start | bytes 1572868
  1.8 1.0 copy-start.4
  2.9 0.7 copy-start.10
  3.6 0.7 copy-start.11
  46.2 1.6 %copy-start.13 = (bf16[1,512,2048]{2,1,0:T(8,128)(2,1)S(1)}, bf16[1,512,2048]{2,1,0:T(8,128)(2,1)}, u32[]{:S(2)}) copy-start(bf16[1,512,2048]{2,1,0:T(8,128)(2,1)} %param.19) | copy-start | bytes 6291460
  57.8 1.6 %copy-start.12 = (bf16[1,2048,512]{2,1,0:T(8,128)(2,1)S(1)}, bf16[1,2048,512]{2,1,0:T(8,128)(2,1)}, u32[]{:S(2)}) copy-start(bf16[1,2048,512]{2,1,0:T(8,128)(2,1)} %param.18) | copy-start | bytes 6291460
  59.3 1.3 %copy-start.2 = (bf16[128,2048]{1,0:T(8,128)(2,1)S(1)}, bf16[128,2048]{1,0:T(8,128)(2,1)}, u32[]{:S(2)}) copy-start(bf16[128,2048]{1,0:T(8,128)(2,1)} %cot_ref.3) | copy-start | bytes 1572868
  59.3 1.4 %copy-start.3 = (bf16[2048,256]{1,0:T(8,128)(2,1)S(1)}, bf16[2048,256]{1,0:T(8,128)(2,1)}, u32[]{:S(2)}) copy-start(bf16[2048,256]{1,0:T(8,128)(2,1)} %proj_ref.1) | copy-start | bytes 3145732
  59.3 1.4 %copy-start.5 = (bf16[256,128]{1,0:T(8,128)(2,1)S(1)}, bf16[256,128]{1,0:T(8,128)(2,1)}, u32[]{:S(2)}) copy-start(bf16[256,128]{1,0:T(8,128)(2,1)} %value_ref.1) | copy-start | bytes 196612
  59.4 1.4 %copy-start.6 = (bf16[256,128]{1,0:T(8,128)(2,1)S(1)}, bf16[256,128]{1,0:T(8,128)(2,1)}, u32[]{:S(2)}) copy-start(bf16[256,128]{1,0:T(8,128)(2,1)} %gate_ref.1) | copy-start | bytes 196612
  59.4 1.4 %copy-start.7 = (bf16[256,128]{1,0:T(8,128)(2,1)S(1)}, bf16[256,128]{1,0:T(8,128)(2,1)}, u32[]{:S(2)}) copy-start(bf16[256,128]{1,0:T(8,128)(2,1)} %conv_ref.1) | copy-start | bytes 196612
  59.4 1.4 %copy-start.8 = (f32[31,256]{1,0:T(8,128)S(1)}, f32[31,256]{1,0:T(8,128)}, u32[]{:S(2)}) copy-start(f32[31,256]{1,0:T(8,128)} %taps_ref.1) | copy-start | bytes 95236
  59.4 1.4 %copy-start.9 = (f32[256]{0:T(256)S(1)}, f32[256]{0:T(256)}, u32[]{:S(2)}) copy-start(f32[256]{0:T(256)} %param.25) | copy-start | bytes 3076

commit v2 on v1

--- a/solution.py
+++ b/solution.py
@@ -52,7 +52,7 @@
 
 def dispatch_kernel(
     n, cap, routes_ref, weights_ref, stream_ref, cot_ref, rows_ref, cots_ref, pick_ref,
-    stage, send_xz, recv_xz, send_y, recv_y, send_c, recv_c, send_d, recv_d,
+    weighted_ref, stage, send_xz, recv_xz, send_y, recv_y, send_c, recv_c, send_d, recv_d,
 ):
     s, q = lax.axis_index("sp"), lax.axis_index("tp")
     q_core, q_y, q_far = partners(q)
@@ -84,6 +84,7 @@
     slot_weight = jnp.sum(weighted, axis=1, keepdims=True)
     pick = pick.astype(bf16)
     pick_ref[...] = pick
+    weighted_ref[...] = weighted
     own = aligned(q * width, width)
     picked = dot(pick, stream_ref[:, own]).astype(bf16)
     stage[0] = picked
@@ -114,10 +115,14 @@
                 for a in range(2)
             ]
         )
-    for a in range(2):
-        outs[a][aligned(s * cap, cap), own] = stage[a, aligned(s * cap, cap), :]
-
-    across, tail = [], []
+    mine = aligned(s * cap, cap)
+    rows_ref[mine, :] = dot(pick_ref[mine, :], stream_ref[...]).astype(bf16)
+    cots_ref[mine, :] = (
+        jnp.sum(weighted_ref[mine, :], axis=1, keepdims=True)
+        * dot(pick_ref[mine, :], cot_ref[...])
+    ).astype(bf16)
+
+    across, tail = [None], []
 
     def far_forward(d):
         source = lax.rem(s + n - d, n)
@@ -132,17 +137,16 @@
                 )
             )
 
-    for d in range(n):
+    for d in range(1, n):
         source = lax.rem(s + n - d, n)
         row = []
         for a in range(2):
-            if d > 0:
-                arriving[d - 1][a].wait_recv()
+            arriving[d - 1][a].wait_recv()
             block = at(a, source, q)
             row.append(start(remote(block, block, send_y.at[a, d], recv_y.at[a, d], s, q_y)))
             tail.append(start(remote(block, block, send_c.at[a, d], recv_c.at[a, d], s, q_core)))
         across.append(row)
-        if d > 0:
+        if d > 1:
             far_forward(d - 1)
     far_forward(n - 1)
     for copy in tail:
@@ -165,7 +169,11 @@
         ),
         in_specs=[pl.BlockSpec(memory_space=pltpu.VMEM)] * 4,
         out_specs=[pl.BlockSpec(memory_space=pltpu.VMEM)] * 3,
-        scratch_shapes=[pltpu.VMEM((2, slots, width), bf16)] + dma,
+        scratch_shapes=[
+            pltpu.VMEM((slots, tokens), f32),
+            pltpu.VMEM((2, slots, width), bf16),
+        ]
+        + dma,
         compiler_params=pltpu.CompilerParams(
             collective_id=0, has_side_effects=True, vmem_limit_bytes=24 << 20
         ),
@@ -429,6 +437,29 @@
     )(part, pick, out_cot, w_proj, value, gate, taps, conv, gain)
 
 
+def flush_kernel(*refs):
+    count = len(refs) // 2
+    copies = [
+        pltpu.make_async_copy(refs[i], refs[count + i], refs[-1].at[i]) for i in range(count)
+    ]
+    for copy in copies:
+        copy.start()
+    for copy in copies:
+        copy.wait()
+
+
+def flush(*arrays):
+    return pl.pallas_call(
+        flush_kernel,
+        out_shape=tuple(jax.ShapeDtypeStruct(a.shape, a.dtype) for a in arrays),
+        in_specs=[pl.BlockSpec(memory_space=pltpu.VMEM)] * len(arrays),
+        out_specs=[pl.BlockSpec(memory_space=pltpu.HBM)] * len(arrays),
+        scratch_shapes=[pltpu.SemaphoreType.DMA((len(arrays),))],
+        compiler_params=pltpu.CompilerParams(vmem_limit_bytes=4 << 20),
+        name="flush",
+    )(*arrays)
+
+
 def expert_terms(rows_in, cot_in, w_gate, w_up, w_down):
     pre_gate = dot(rows_in, w_gate)
     pre_up = dot(rows_in, w_up)
@@ -469,6 +500,9 @@
     grad_stream, grad_proj, grad_value, grad_gate_in = tail(
         part, pick, out_cot, w_proj, conv_value, conv_gate, conv_taps, conv_result,
         channel_norm_gain[None, :], n, cap, tp_count,
+    )
+    grad_stream, grad_proj, grad_value, grad_gate_in = flush(
+        grad_stream, grad_proj, grad_value, grad_gate_in
     )
     return (
         grad_gate[None], grad_up[None], grad_down[None],

time: 109 us -> 107 us (0.982)
  local copies, waits for them, and re-layouts: 7.03 us -> 4.28 us
    unnamed x32 -> x28, local copies, waits for them, and re-layouts: 7.03 us -> 4.28 us
where the time goes in v2:
time: 107 us
  Pallas kernels  84.9 us (79%)
  matrix products  16.6 us (16%)
  local copies, waits for them, and re-layouts  4.28 us (4%)
    pallas_call x1, Pallas kernels, tail(): pl.pallas_call(functools.partial(tail_kernel, n, cap, channels * tp_count...  44.9 us
    pallas_call x1, Pallas kernels, dispatch(): pl.pallas_call(functools.partial(dispatch_kernel, n, cap), out_shape=(jax...  39.1 us
    dot_general x8, matrix products, dot(): lax.dot_general(a, b, (((ca,), (cb,)), ((), ())), preferred_element_type=...  16.6 us
    unnamed x28, local copies, waits for them, and re-layouts  4.28 us

profile of v2, /device:TPU:0, one launch (start us, length us, event | category | flops | bytes accessed | tf_op | source)
XLA Modules:
  0.0 106.6 jit_solution(1000961606898393555)
XLA Ops:
  0.6 0.0 copy-start
  0.6 0.0 copy-start.1
  0.7 1.2 %copy-done.1 = bf16[128,2048]{1,0:T(8,128)(2,1)S(1)} copy-done((bf16[128,2048]{1,0:T(8,128)(2,1)S(1)}, bf16[128,2048]{1,0:T(8,128)(2,1)}, u32[]{:S(2)}) %copy-start.1) | copy-done | bytes 524312
  1.8 0.0 copy-start.4
  1.8 1.0 copy-done.4
  2.9 0.0 copy-start.10
  2.9 0.7 copy-done.10
  3.6 0.0 copy-start.11
  3.6 0.7 copy-done.11
  4.2 39.1 %dispatch.1 = (bf16[512,2048]{1,0:T(8,128)(2,1)S(1)}, bf16[512,2048]{1,0:T(8,128)(2,1)S(1)}, bf16[512,128]{1,0:T(8,128)(2,1)S(1)}) custom-call(s32[2,128]{1,0:T(2,128)S(1)} %bitcast.35, f32[2,128]{1,0:T(2,128)S(1)} %bitcast.36, bf16[128,2048]{1,0:T(8,128)(2,1)S(1)} %copy-done.4, bf16[128,2048]{1,0:T(8,128)(2,1)S(1)} %copy-done.1), custom_call_target="tpu_custom_call" | custom-call | tf_op jit(solution)/shard_map/dispatch/pallas_call | solution.py:163
  43.3 2.8 %fusion.4 = f32[512,512]{1,0:T(8,128)S(1)} fusion(bf16[512,2048]{1,0:T(8,128)(2,1)S(1)} %get-tuple-element.18, bf16[1,2048,512]{2,1,0:T(8,128)(2,1)} %param.18), kind=kOutput, calls=%fused_computation.8 | convolution fusion | flops 1073741824 | bytes 5242880 | tf_op jit(solution)/shard_map/dot_general | solution.py:19
  46.2 0.0 copy-done
  46.2 0.0 copy-start.13
  46.2 1.2 %fusion.10 = f32[512,512]{1,0:T(8,128)S(1)} fusion(bf16[512,2048]{1,0:T(8,128)(2,1)S(1)} %get-tuple-element.18, bf16[1,2048,512]{2,1,0:T(8,128)(2,1)S(1)} %copy-done), kind=kOutput, calls=%fused_computation.14 | convolution fusion | flops 1073741824 | bytes 5242880 | tf_op jit(solution)/shard_map/dot_general | solution.py:19
  47.4 0.3 copy-done.13
  47.8 1.9 %select_convert_fusion = (bf16[512,512]{1,0:T(8,128)(2,1)S(1)}, bf16[512,512]{1,0:T(8,128)(2,1)S(1)}) fusion(f32[512,512]{1,0:T(8,128)S(1)} %fusion.4, f32[512,512]{1,0:T(8,128)S(1)} %fusion.10, bf16[512,2048]{1,0:T(8,128)(2,1)S(1)} %get-tuple-element.19, bf16[1,512,2048]{2,1,0:T(8,128)(2,1)S(1)} %copy-done.13), kind=kOutput, calls=%fused_computation.17 | convolution fusion | flops 1079508992 | bytes 7340032 | tf_op jit(solution)/shard_map/dot_general | solution.py:19
  49.7 2.8 %fusion.2 = bf16[1,512,2048]{2,1,0:T(8,128)(2,1)} fusion(bf16[512,2048]{1,0:T(8,128)(2,1)S(1)} %get-tuple-element.19, f32[512,512]{1,0:T(8,128)S(1)} %fusion.10, f32[512,512]{1,0:T(8,128)S(1)} %fusion.4), kind=kOutput, calls=%fused_computation.6 | convolution fusion | flops 1077411840 | bytes 6291456 | tf_op jit(solution)/shard_map/dot_general | solution.py:19
  52.5 2.6 %fusion.1 = bf16[1,2048,512]{2,1,0:T(8,128)(2,1)} fusion(bf16[512,2048]{1,0:T(8,128)(2,1)S(1)} %get-tuple-element.18, bf16[512,512]{1,0:T(8,128)(2,1)S(1)} %get-tuple-element.29), kind=kOutput, calls=%fused_computation.5 | convolution fusion | flops 1074790400 | bytes 4718592 | tf_op jit(solution)/shard_map/dot_general | solution.py:19
  55.1 2.6 %fusion = bf16[1,2048,512]{2,1,0:T(8,128)(2,1)} fusion(bf16[512,2048]{1,0:T(8,128)(2,1)S(1)} %get-tuple-element.18, bf16[512,512]{1,0:T(8,128)(2,1)S(1)} %get-tuple-element.30), kind=kOutput, calls=%fused_computation.4 | convolution fusion | flops 1074790400 | bytes 4718592 | tf_op jit(solution)/shard_map/dot_general | solution.py:19
  57.7 0.0 copy-start.12
  57.7 1.3 %fusion.8 = f32[512,2048]{1,0:T(8,128)S(1)} fusion(bf16[512,512]{1,0:T(8,128)(2,1)S(1)} %get-tuple-element.30, bf16[1,2048,512]{2,1,0:T(8,128)(2,1)S(1)} %copy-done), kind=kOutput, calls=%fused_computation.12 | convolution fusion | flops 1073741824 | bytes 6815744 | tf_op jit(solution)/shard_map/dot_general | solution.py:19
  59.0 0.3 copy-done.12
  59.3 0.0 copy-start.2
  59.3 0.0 copy-start.3
  59.3 0.0 copy-start.5
  59.3 0.0 copy-start.6
  59.3 0.0 copy-start.7
  59.3 0.0 copy-start.8
  59.3 0.0 copy-start.9
  59.4 1.3 %add_convert_fusion.part_ref = bf16[512,2048]{1,0:T(8,128)(2,1)S(1)} fusion(f32[512,2048]{1,0:T(8,128)S(1)} %fusion.8, bf16[512,512]{1,0:T(8,128)(2,1)S(1)} %get-tuple-element.29, bf16[1,2048,512]{2,1,0:T(8,128)(2,1)S(1)} %copy-done.12), kind=kOutput, calls=%fused_computation | convolution fusion | flops 1075838976 | bytes 8912896 | tf_op jit(solution)/shard_map/dot_general | solution.py:19
  60.7 0.0 copy-done.2
  60.7 0.0 copy-done.3
  60.7 0.0 copy-done.5
  60.7 0.0 copy-done.6
  60.7 0.0 copy-done.7
  60.7 0.0 copy-done.8
  60.7 0.0 copy-done.9
  60.7 44.9 %combine_tail.1 = (bf16[128,2048]{1,0:T(8,128)(2,1)S(1)}, f32[256,256]{1,0:T(8,128)S(1)}, bf16[256,128]{1,0:T(8,128)(2,1)S(1)}, bf16[256,128]{1,0:T(8,128)(2,1)S(1)}) custom-call(bf16[512,2048]{1,0:T(8,128)(2,1)S(1)} %add_convert_fusion.part_ref, bf16[512,128]{1,0:T(8,128)(2,1)S(1)} %get-tuple-element.20.pick_ref, bf16[128,2048]{1,0:T(8,128)(2,1)S(1)} %copy-done.2, ...), custom_call_target="tpu_custom_call" | custom-call | tf_op jit(solution)/shard_map/combine_tail/pallas_call | solution.py:409
  105.6 0.9 flush.1
Async XLA Ops:
  0.6 45.5 %copy-start = (bf16[1,2048,512]{2,1,0:T(8,128)(2,1)S(1)}, bf16[1,2048,512]{2,1,0:T(8,128)(2,1)}, u32[]{:S(2)}) copy-start(bf16[1,2048,512]{2,1,0:T(8,128)(2,1)} %param.17) | copy-start | bytes 6291460
  0.6 1.2 %copy-start.1 = (bf16[128,2048]{1,0:T(8,128)(2,1)S(1)}, bf16[128,2048]{1,0:T(8,128)(2,1)}, u32[]{:S(2)}) copy-start(bf16[128,2048]{1,0:T(8,128)(2,1)} %cot_ref.3) | copy-start | bytes 1572868
  1.8 1.0 copy-start.4
  2.9 0.7 copy-start.10
  3.6 0.7 copy-start.11
  46.2 1.6 %copy-start.13 = (bf16[1,512,2048]{2,1,0:T(8,128)(2,1)S(1)}, bf16[1,512,2048]{2,1,0:T(8,128)(2,1)}, u32[]{:S(2)}) copy-start(bf16[1,512,2048]{2,1,0:T(8,128)(2,1)} %param.19) | copy-start | bytes 6291460
  57.7 1.6 %copy-start.12 = (bf16[1,2048,512]{2,1,0:T(8,128)(2,1)S(1)}, bf16[1,2048,512]{2,1,0:T(8,128)(2,1)}, u32[]{:S(2)}) copy-start(bf16[1,2048,512]{2,1,0:T(8,128)(2,1)} %param.18) | copy-start | bytes 6291460
  59.3 1.3 %copy-start.2 = (bf16[128,2048]{1,0:T(8,128)(2,1)S(1)}, bf16[128,2048]{1,0:T(8,128)(2,1)}, u32[]{:S(2)}) copy-start(bf16[128,2048]{1,0:T(8,128)(2,1)} %cot_ref.3) | copy-start | bytes 1572868
  59.3 1.4 %copy-start.3 = (bf16[2048,256]{1,0:T(8,128)(2,1)S(1)}, bf16[2048,256]{1,0:T(8,128)(2,1)}, u32[]{:S(2)}) copy-start(bf16[2048,256]{1,0:T(8,128)(2,1)} %proj_ref.1) | copy-start | bytes 3145732
  59.3 1.4 %copy-start.5 = (bf16[256,128]{1,0:T(8,128)(2,1)S(1)}, bf16[256,128]{1,0:T(8,128)(2,1)}, u32[]{:S(2)}) copy-start(bf16[256,128]{1,0:T(8,128)(2,1)} %value_ref.1) | copy-start | bytes 196612
  59.3 1.4 %copy-start.6 = (bf16[256,128]{1,0:T(8,128)(2,1)S(1)}, bf16[256,128]{1,0:T(8,128)(2,1)}, u32[]{:S(2)}) copy-start(bf16[256,128]{1,0:T(8,128)(2,1)} %gate_ref.1) | copy-start | bytes 196612
  59.3 1.4 %copy-start.7 = (bf16[256,128]{1,0:T(8,128)(2,1)S(1)}, bf16[256,128]{1,0:T(8,128)(2,1)}, u32[]{:S(2)}) copy-start(bf16[256,128]{1,0:T(8,128)(2,1)} %conv_ref.1) | copy-start | bytes 196612
  59.3 1.4 %copy-start.8 = (f32[31,256]{1,0:T(8,128)S(1)}, f32[31,256]{1,0:T(8,128)}, u32[]{:S(2)}) copy-start(f32[31,256]{1,0:T(8,128)} %taps_ref.1) | copy-start | bytes 95236
  59.3 1.4 %copy-start.9 = (f32[256]{0:T(256)S(1)}, f32[256]{0:T(256)}, u32[]{:S(2)}) copy-start(f32[256]{0:T(256)} %param.25) | copy-start | bytes 3076
